TPU v7x, 256 devices: a whole 4x4x8 slice. The times are simulated.
256 devices in a mesh: fs: 32 (over z, y), tp: 8 (over x, core).
Axes of the slice: x: 4, y: 4, z: 8, core: 2. Of those that a mesh axis runs over, the one named last changes fastest.
Arguments:
- prompt: bfloat16 [32768, 2048], P(('fs', 'tp')), may hold values from -6 to 6
- norm_gain: float32 [2048], P('fs'), may hold values from 0.1 to 1.9
- up_trained: float32 [2048, 8192], P('fs', 'tp'), may hold values from -0.125 to 0.125
- down_trained: float32 [2048, 8192], P('fs', 'tp'), may hold values from -0.0625 to 0.0625
Outputs:
- up_served: bfloat16 [2048, 8192], P(None, 'tp')
- down_served: bfloat16 [8192, 2048], P('tp')
- mixed: bfloat16 [32768, 2048], P(('fs', 'tp'))
All inputs are finite; a program needn't handle non-finite values.
Results may differ from a plain program's by a relative error of at most 0.014.
Values may be sent and summed in bfloat16 or wider, within the bound.
No kernel may reach another device: no remote copies, remote signals or barrier semaphores. Data moves between devices by JAX's collectives and lax.ppermute only.
A program may use at most 128 MiB of HBM per device.

v0:
```python
import jax
import jax.numpy as jnp
from jax import lax
from jax.sharding import PartitionSpec as P


def sent_together(arrays, axis, dim, along):
    both = jnp.concatenate(arrays, axis=along)
    filled, at, finished = (lax.all_gather(both, axis, axis=dim, tiled=True), 0, [])
    for a in arrays:
        finished.append(lax.slice_in_dim(filled, at, at + a.shape[along], axis=along))
        at += a.shape[along]
    return tuple(finished)


def shards(prompt, norm_gain, up_trained, down_trained):
    up_local = (norm_gain[:, None] * up_trained).astype(jnp.bfloat16)
    down_local = down_trained.astype(jnp.bfloat16)
    values = prompt.astype(jnp.float32)
    scale = lax.rsqrt(jnp.mean(values * values, axis=-1, keepdims=True) + 1e-06)
    normed = (values * scale).astype(jnp.bfloat16)
    group_rows = lax.all_gather(normed, "tp", axis=0, tiled=True)
    up_whole, down_whole = sent_together((up_local, down_local), "fs", 0, 1)
    pre = jnp.dot(group_rows, up_whole, preferred_element_type=jnp.float32)
    hidden = jnp.square(jax.nn.relu(pre)).astype(jnp.bfloat16)
    down_served = jnp.transpose(down_whole)
    mixed = lax.psum_scatter(
        jnp.dot(hidden, down_served, preferred_element_type=jnp.float32).astype(jnp.bfloat16),
        "tp",
        scatter_dimension=0,
        tiled=True,
    )
    return (up_whole, down_served, mixed)


def solution(mesh):
    return jax.shard_map(
        shards,
        mesh=mesh,
        in_specs=(P(("fs", "tp"), None), P("fs"), P("fs", "tp"), P("fs", "tp")),
        out_specs=(P(None, "tp"), P("tp", None), P(("fs", "tp"), None)),
        check_vma=False,
    )
```

profile of v0, /device:TPU:8, one launch (start us, length us, event | category | flops | bytes accessed | tf_op | source)
XLA Modules:
  0.0 207.6 jit_solution(5565873400041753207)
XLA Ops:
  7.2 0.0 all-gather.3.cloned.1.call-start
  7.2 1.0 convert_element_type.19
  8.2 1.0 multiply_convert_fusion.1
  9.2 0.7 pad_maximum_fusion
  9.9 0.0 all-gather.3.cloned.1.call-update
  10.0 0.0 all-gather.5.cloned.1.call-start
  10.0 1.2 fusion.1
  11.3 2.0 fusion.2
  13.2 0.0 all-gather.5.cloned.1.call-update
  13.3 0.0 reduce-scatter.2.cloned.1.call-start
  13.3 97.3 %all-gather.3.cloned.1.call-done = bf16[2048,2048]{1,0:T(8,128)(2,1)} async-done(((bf16[64,2048]{1,0:T(8,128)(2,1)}), bf16[2048,2048]{1,0:T(8,128)(2,1)}) %all-gather.3.cloned.1.call-update) | async-done | bytes 8388624 | tf_op jit(solution)/shard_map/all_gather | solution.py:9
  110.7 6.0 %slice_bitcast_fusion = (bf16[1024,2048]{0,1:T(8,128)(2,1)}, bf16[2048,1024]{1,0:T(8,128)(2,1)}) fusion(bf16[2048,2048]{1,0:T(8,128)(2,1)} %all-gather.3.cloned.1.call-done), kind=kLoop, calls=%fused_computation.3 | loop fusion | bytes 16777216 | tf_op jit(solution)/shard_map/transpose | solution.py:26
  116.7 29.4 %all-gather.5.cloned.1.call-done = bf16[1024,2048]{1,0:T(8,128)(2,1)} async-done(((bf16[128,2048]{1,0:T(8,128)(2,1)}), bf16[1024,2048]{1,0:T(8,128)(2,1)}) %all-gather.5.cloned.1.call-update) | async-done | bytes 4194320 | tf_op jit(solution)/shard_map/all_gather | solution.py:22
  146.0 14.4 %convolution_convert_fusion = bf16[1024,2048]{1,0:T(8,128)(2,1)} fusion(bf16[2048,2048]{1,0:T(8,128)(2,1)} %all-gather.3.cloned.1.call-done, bf16[1024,2048]{1,0:T(8,128)(2,1)} %all-gather.5.cloned.1.call-done, bf16[2048,1024]{1,0:T(8,128)(2,1)} %get-tuple-element.10), kind=kOutput, calls=%fused_computation.1 | convolution fusion | flops 8595177472 | bytes 16777216 | tf_op jit(solution)/shard_map/dot_general | solution.py:28
  160.4 0.0 reduce-scatter.2.cloned.1.call-update
  160.4 6.4 %copy.10 = bf16[1024,2048]{1,0:T(8,128)(2,1)} copy(bf16[1024,2048]{0,1:T(8,128)(2,1)} %get-tuple-element.9) | data formatting | bytes 8388608
  166.9 34.2 %reduce-scatter.2.cloned.1.call-done = bf16[128,2048]{1,0:T(8,128)(2,1)} async-done(((bf16[1024,2048]{1,0:T(8,128)(2,1)}), bf16[128,2048]{1,0:T(8,128)(2,1)}) %reduce-scatter.2.cloned.1.call-update) | async-done | bytes 524304 | tf_op jit(solution)/shard_map/reduce_scatter | solution.py:27
  (1 shorter events, 0.0 us)
Async XLA Ops:
  7.2 103.5 %all-gather.3.cloned.1.call-start = ((), (), s32[]{:S(2)}) async-start(), calls=%async_computation.1 | async-start | bytes 8650752 | tf_op jit(solution)/shard_map/all_gather | solution.py:9
  10.0 136.1 %all-gather.5.cloned.1.call-start = ((), (), s32[]{:S(2)}) async-start(), calls=%async_computation.2 | async-start | bytes 4718592 | tf_op jit(solution)/shard_map/all_gather | solution.py:22
  13.3 187.8 %reduce-scatter.2.cloned.1.call-start = ((), (), s32[]{:S(2)}) async-start(), calls=%async_computation.3 | async-start | bytes 4718592 | tf_op jit(solution)/shard_map/reduce_scatter | solution.py:27
Sparse Core Ops, SparseCore 0:
  11.1 99.4 all-gather.2
  113.1 32.8 all-gather.4
  160.5 40.4 reduce-scatter.1
where the time goes:
time: 208 us
  waiting for transfers between devices  161 us (77%)
  matrix products  14.4 us (7%)
  between operations  13.8 us (7%)
  local copies, waits for them, and re-layouts  12.5 us (6%)
  other arithmetic  5.96 us (3%)
    all_gather x1, waiting for transfers between devices, sent_together(): lax.all_gather(both, axis, axis=dim, tiled=True)  97.3 us
    reduce_scatter x1, waiting for transfers between devices, shards(): lax.psum_scatter(jnp.dot(hidden, down_served, preferred_element_type=jnp....  34.2 us
    all_gather x1, waiting for transfers between devices, shards(): group_rows = lax.all_gather(normed, 'tp', axis=0, tiled=True)  29.4 us
    dot_general x1, matrix products, shards(): jnp.dot(hidden, down_served, preferred_element_type=jnp.float32)  14.4 us
    unnamed x1, local copies, waits for them, and re-layouts  6.43 us
    transpose x1, local copies, waits for them, and re-layouts, shards(): down_served = jnp.transpose(down_whole)  6.02 us
  transfers between devices with their start and end apart: 3, of which 3 were waited for; matrix products, arithmetic and copies ran while one was open for 8% of the time, Pallas kernels for 0%

commit v1 on v0

--- a/solution.py
+++ b/solution.py
@@ -2,6 +2,12 @@
 import jax.numpy as jnp
 from jax import lax
 from jax.sharding import PartitionSpec as P
+
+
+def mark_run_by_axis(arr_in, d0):
+    back = list(arr_in.shape[1:])
+    back[d0] *= arr_in.shape[0]
+    return jnp.moveaxis(arr_in, 0, d0).reshape(back)
 
 
 def sent_together(arrays, axis, dim, along):
@@ -19,7 +25,34 @@
     values = prompt.astype(jnp.float32)
     scale = lax.rsqrt(jnp.mean(values * values, axis=-1, keepdims=True) + 1e-06)
     normed = (values * scale).astype(jnp.bfloat16)
-    group_rows = lax.all_gather(normed, "tp", axis=0, tiled=True)
+
+    def make_limits(out_dim, comm_axis, tile_in):
+        degree = lax.axis_size(comm_axis)
+        val2 = map(lambda ix: (ix, (ix + 1) % degree), range(degree))
+        frames = list(val2)
+        samples = [(p, kk) for kk, p in frames]
+        current_value, moved = ([], [])
+        for no in [*range(degree - 1)]:
+            if no % 2 == 0:
+                local_next = lax.ppermute(
+                    current_value[-1] if current_value else tile_in,
+                    axis_name=comm_axis,
+                    perm=frames,
+                )
+                current_value.append(local_next)
+            else:
+                v1 = lax.ppermute(
+                    moved[-1] if moved else tile_in, perm=samples, axis_name=comm_axis
+                )
+                moved.append(v1)
+        view_out = jnp.stack([*current_value[::-1], tile_in, *moved], axis=0)
+        current_block = lax.axis_index(comm_axis)
+        earlier = len(current_value)
+        fresh = current_block - earlier
+        view_out = view_out[(jnp.arange(degree) - fresh) % degree]
+        return mark_run_by_axis(view_out, out_dim)
+
+    group_rows = make_limits(0, "tp", normed)
     up_whole, down_whole = sent_together((up_local, down_local), "fs", 0, 1)
     pre = jnp.dot(group_rows, up_whole, preferred_element_type=jnp.float32)
     hidden = jnp.square(jax.nn.relu(pre)).astype(jnp.bfloat16)

time: 208 us -> 177 us (0.85)
  waiting for transfers between devices: 161 us -> 108 us
  local copies, waits for them, and re-layouts: 12.5 us -> 24.3 us
  starting transfers between devices: 0.12 us -> 9.48 us
    all_gather x1, waiting for transfers between devices: 97.3 us -> 46 us  [sent_together(): lax.all_gather(both, axis, axis=dim, tiled=True)]
    ppermute x0 -> x7, waiting for transfers between devices: none -> 29.9 us  [the longest x4 29.9 us: make_limits(): lax.ppermute(current_value[-1] if current_value else tile_in, axis_name=c...]
    all_gather x1 -> x0, waiting for transfers between devices: 29.4 us -> none  [shards(): group_rows = lax.all_gather(normed, 'tp', axis=0, tiled=True)]
    ppermute x0 -> x7, starting transfers between devices: none -> 9.4 us  [the longest x3 9.38 us: make_limits(): lax.ppermute(moved[-1] if moved else tile_in, perm=samples, axis_name=com...]
    unnamed x1 -> x9, local copies, waits for them, and re-layouts: 6.43 us -> 12.5 us
    gather x0 -> x1, local copies, waits for them, and re-layouts: none -> 4.93 us  [make_limits(): view_out = view_out[(jnp.arange(degree) - fresh) % degree]]
  transfers between devices with their start and end apart: 3 -> 9, of which waited for: 3 -> 6; matrix products, arithmetic and copies ran while one was open for 8% -> 12% of each run, Pallas kernels for 0% -> 0%
where the time goes in v1:
time: 177 us
  waiting for transfers between devices  108 us (61%)
  local copies, waits for them, and re-layouts  24.3 us (14%)
  matrix products  14.4 us (8%)
  between operations  14.1 us (8%)
  starting transfers between devices  9.48 us (5%)
  other arithmetic  6.18 us (3%)
    all_gather x1, waiting for transfers between devices, sent_together(): lax.all_gather(both, axis, axis=dim, tiled=True)  46 us
    reduce_scatter x1, waiting for transfers between devices, shards(): lax.psum_scatter(jnp.dot(hidden, down_served, preferred_element_type=jnp....  32.5 us
    ppermute x4, waiting for transfers between devices, make_limits(): lax.ppermute(current_value[-1] if current_value else tile_in, axis_name=c...  29.9 us
    dot_general x1, matrix products, shards(): jnp.dot(hidden, down_served, preferred_element_type=jnp.float32)  14.4 us
    unnamed x9, local copies, waits for them, and re-layouts  12.5 us
    ppermute x3, starting transfers between devices, make_limits(): lax.ppermute(moved[-1] if moved else tile_in, perm=samples, axis_name=com...  9.38 us
    transpose x1, local copies, waits for them, and re-layouts, shards(): down_served = jnp.transpose(down_whole)  6.02 us
    gather x1, local copies, waits for them, and re-layouts, make_limits(): view_out = view_out[(jnp.arange(degree) - fresh) % degree]  4.93 us
  transfers between devices with their start and end apart: 9, of which 6 were waited for; matrix products, arithmetic and copies ran while one was open for 12% of the time, Pallas kernels for 0%

profile of v1, /device:TPU:8, one launch (start us, length us, event | category | flops | bytes accessed | tf_op | source)
XLA Modules:
  0.0 176.8 jit_solution(523667266975837938)
XLA Ops:
  7.2 0.0 copy-start
  7.2 0.0 all-gather.2.cloned.1.call-start
  7.2 1.0 convert_element_type.19
  8.2 1.0 multiply_convert_fusion.1
  9.3 0.7 pad_maximum_fusion
  10.0 0.0 all-gather.2.cloned.1.call-update
  10.0 0.0 reduce-scatter.2.cloned.1.call-start
  10.1 1.2 fusion.1
  11.3 1.2 fusion.2
  12.5 0.0 collective-permute-start
  12.5 9.8 %collective-permute-done = bf16[128,2048]{1,0:T(8,128)(2,1)S(1)} collective-permute-done((bf16[128,2048]{1,0:T(8,128)(2,1)S(1)}, bf16[128,2048]{1,0:T(8,128)(2,1)S(1)}, u32[]{:S(2)}, u32[]{:S(2)}) %collective-permute-start) | collective-permute-done | bytes 524320 | tf_op jit(solution)/shard_map/ppermute | solution.py:37
  22.4 3.0 %collective-permute-start.4 = (bf16[128,2048]{1,0:T(8,128)(2,1)S(1)}, bf16[128,2048]{1,0:T(8,128)(2,1)S(1)}, u32[]{:S(2)}, u32[]{:S(2)}) collective-permute-start(bf16[128,2048]{1,0:T(8,128)(2,1)S(1)} %fusion.2), channel_id=1, source_target_pairs={{1,0},{2,1},{3,2},{4,3},{5,4},{6,5},{7,6},{0,7},{9,8},{10,9},{11,1... | collective-permute-start | bytes 1572872 | tf_op jit(solution)/shard_map/ppermute | solution.py:44
  25.3 6.9 %collective-permute-done.1 = bf16[128,2048]{1,0:T(8,128)(2,1)S(1)} collective-permute-done((bf16[128,2048]{1,0:T(8,128)(2,1)S(1)}, bf16[128,2048]{1,0:T(8,128)(2,1)S(1)}, u32[]{:S(2)}, u32[]{:S(2)}) %collective-permute-start.1) | collective-permute-done | bytes 524320 | tf_op jit(solution)/shard_map/ppermute | solution.py:37
  32.2 3.0 %collective-permute-start.5 = (bf16[128,2048]{1,0:T(8,128)(2,1)S(1)}, bf16[128,2048]{1,0:T(8,128)(2,1)S(1)}, u32[]{:S(2)}, u32[]{:S(2)}) collective-permute-start(bf16[128,2048]{1,0:T(8,128)(2,1)S(1)} %collective-permute-done.4), channel_id=1, source_target_pairs={{1,0},{2,1},{3,2},{4,3},{5,4},{6,5},{7,6},{0,7},{9,8},{10,9},{11,1... | collective-permute-start | bytes 1572872 | tf_op jit(solution)/shard_map/ppermute | solution.py:44
  35.2 6.8 %collective-permute-done.2 = bf16[128,2048]{1,0:T(8,128)(2,1)S(1)} collective-permute-done((bf16[128,2048]{1,0:T(8,128)(2,1)S(1)}, bf16[128,2048]{1,0:T(8,128)(2,1)S(1)}, u32[]{:S(2)}, u32[]{:S(2)}) %collective-permute-start.2) | collective-permute-done | bytes 524320 | tf_op jit(solution)/shard_map/ppermute | solution.py:37
  42.0 3.4 %collective-permute-start.6 = (bf16[128,2048]{1,0:T(8,128)(2,1)S(1)}, bf16[128,2048]{1,0:T(8,128)(2,1)S(1)}, u32[]{:S(2)}, u32[]{:S(2)}) collective-permute-start(bf16[128,2048]{1,0:T(8,128)(2,1)S(1)} %collective-permute-done.5), channel_id=1, source_target_pairs={{1,0},{2,1},{3,2},{4,3},{5,4},{6,5},{7,6},{0,7},{9,8},{10,9},{11,1... | collective-permute-start | bytes 1572872 | tf_op jit(solution)/shard_map/ppermute | solution.py:44
  45.4 6.5 %collective-permute-done.3 = bf16[128,2048]{1,0:T(8,128)(2,1)} collective-permute-done((bf16[128,2048]{1,0:T(8,128)(2,1)S(1)}, bf16[128,2048]{1,0:T(8,128)(2,1)}, u32[]{:S(2)}, u32[]{:S(2)}) %collective-permute-start.3) | collective-permute-done | bytes 524320 | tf_op jit(solution)/shard_map/ppermute | solution.py:37
  51.9 1.9 %bitcast_dynamic-update-slice_fusion.7 = bf16[8,128,2048]{2,1,0:T(8,128)(2,1)} fusion(bf16[128,2048]{1,0:T(8,128)(2,1)} %collective-permute-done.3), kind=kLoop, calls=%fused_computation.16 | loop fusion | bytes 1048576
  53.8 0.8 bitcast_dynamic-update-slice_fusion.6
  54.6 0.8 bitcast_dynamic-update-slice_fusion.5
  55.4 0.8 bitcast_dynamic-update-slice_fusion.4
  56.3 0.9 bitcast_dynamic-update-slice_fusion.3
  57.2 0.8 bitcast_dynamic-update-slice_fusion.2
  58.1 0.8 bitcast_dynamic-update-slice_fusion.1
  58.9 0.8 bitcast_dynamic-update-slice_fusion
  59.7 4.9 %gather_fusion = bf16[8,128,2048]{2,1,0:T(8,128)(2,1)} fusion(bf16[8,128,2048]{2,1,0:T(8,128)(2,1)} %bitcast_dynamic-update-slice_fusion, s32[1024]{0:T(1024)S(1)} %pad_clamp_fusion), kind=kCustom, calls=%fused_computation | custom fusion | bytes 8388640 | tf_op jit(solution)/shard_map/gather | solution.py:52
  64.7 46.0 %all-gather.2.cloned.1.call-done = bf16[2048,2048]{1,0:T(8,128)(2,1)} async-done(((bf16[64,2048]{1,0:T(8,128)(2,1)}), bf16[2048,2048]{1,0:T(8,128)(2,1)}) %all-gather.2.cloned.1.call-update) | async-done | bytes 8388624 | tf_op jit(solution)/shard_map/all_gather | solution.py:15
  110.7 6.0 %slice_bitcast_fusion = (bf16[1024,2048]{0,1:T(8,128)(2,1)}, bf16[2048,1024]{1,0:T(8,128)(2,1)}) fusion(bf16[2048,2048]{1,0:T(8,128)(2,1)} %all-gather.2.cloned.1.call-done), kind=kLoop, calls=%fused_computation.4 | loop fusion | bytes 16777216 | tf_op jit(solution)/shard_map/transpose | solution.py:59
  116.7 14.4 %convolution_convert_fusion = bf16[1024,2048]{1,0:T(8,128)(2,1)} fusion(bf16[2048,2048]{1,0:T(8,128)(2,1)} %all-gather.2.cloned.1.call-done, bf16[1024,2048]{1,0:T(8,128)(2,1)} %bitcast.23, bf16[2048,1024]{1,0:T(8,128)(2,1)} %get-tuple-element.10), kind=kOutput, calls=%fused_computation.2 | convolution fusion | flops 8595177472 | bytes 16777216 | tf_op jit(solution)/shard_map/dot_general | solution.py:61
  131.1 0.0 reduce-scatter.2.cloned.1.call-update
  131.1 6.4 %copy.10 = bf16[1024,2048]{1,0:T(8,128)(2,1)} copy(bf16[1024,2048]{0,1:T(8,128)(2,1)} %get-tuple-element.9) | data formatting | bytes 8388608
  137.5 32.5 %reduce-scatter.2.cloned.1.call-done = bf16[128,2048]{1,0:T(8,128)(2,1)} async-done(((bf16[1024,2048]{1,0:T(8,128)(2,1)}), bf16[128,2048]{1,0:T(8,128)(2,1)}) %reduce-scatter.2.cloned.1.call-update) | async-done | bytes 524304 | tf_op jit(solution)/shard_map/reduce_scatter | solution.py:60
  (10 shorter events, 0.0 us)
Async XLA Ops:
  7.2 49.1 %copy-start = (bf16[128,2048]{1,0:T(8,128)(2,1)S(1)}, bf16[128,2048]{1,0:T(8,128)(2,1)}, u32[]{:S(2)}) copy-start(bf16[128,2048]{1,0:T(8,128)(2,1)} %param.4) | copy-start | bytes 1572868
  7.2 103.5 %all-gather.2.cloned.1.call-start = ((), (), s32[]{:S(2)}) async-start(), calls=%async_computation.1 | async-start | bytes 8650752 | tf_op jit(solution)/shard_map/all_gather | solution.py:15
  10.0 160.0 %reduce-scatter.2.cloned.1.call-start = ((), (), s32[]{:S(2)}) async-start(), calls=%async_computation.2 | async-start | bytes 4718592 | tf_op jit(solution)/shard_map/reduce_scatter | solution.py:60
  12.5 9.8 %collective-permute-start = (bf16[128,2048]{1,0:T(8,128)(2,1)S(1)}, bf16[128,2048]{1,0:T(8,128)(2,1)S(1)}, u32[]{:S(2)}, u32[]{:S(2)}) collective-permute-start(bf16[128,2048]{1,0:T(8,128)(2,1)S(1)} %fusion.2), channel_id=1, source_target_pairs={{0,1},{1,2},{2,3},{3,4},{4,5},{5,6},{6,7},{7,0},{8,9},{9,10},{10,1... | collective-permute-start | bytes 1572872 | tf_op jit(solution)/shard_map/ppermute | solution.py:37
  22.3 9.8 %collective-permute-start.1 = (bf16[128,2048]{1,0:T(8,128)(2,1)S(1)}, bf16[128,2048]{1,0:T(8,128)(2,1)S(1)}, u32[]{:S(2)}, u32[]{:S(2)}) collective-permute-start(bf16[128,2048]{1,0:T(8,128)(2,1)S(1)} %collective-permute-done), channel_id=1, source_target_pairs={{0,1},{1,2},{2,3},{3,4},{4,5},{5,6},{6,7},{7,0},{8,9},{9,10},{10,1... | collective-permute-start | bytes 1572872 | tf_op jit(solution)/shard_map/ppermute | solution.py:37
  22.4 9.8 %collective-permute-start.4 = (bf16[128,2048]{1,0:T(8,128)(2,1)S(1)}, bf16[128,2048]{1,0:T(8,128)(2,1)S(1)}, u32[]{:S(2)}, u32[]{:S(2)}) collective-permute-start(bf16[128,2048]{1,0:T(8,128)(2,1)S(1)} %fusion.2), channel_id=1, source_target_pairs={{1,0},{2,1},{3,2},{4,3},{5,4},{6,5},{7,6},{0,7},{9,8},{10,9},{11,1... | collective-permute-start | bytes 1572872 | tf_op jit(solution)/shard_map/ppermute | solution.py:44
  32.2 9.8 %collective-permute-start.2 = (bf16[128,2048]{1,0:T(8,128)(2,1)S(1)}, bf16[128,2048]{1,0:T(8,128)(2,1)S(1)}, u32[]{:S(2)}, u32[]{:S(2)}) collective-permute-start(bf16[128,2048]{1,0:T(8,128)(2,1)S(1)} %collective-permute-done.1), channel_id=1, source_target_pairs={{0,1},{1,2},{2,3},{3,4},{4,5},{5,6},{6,7},{7,0},{8,9},{9,10},{10,1... | collective-permute-start | bytes 1572872 | tf_op jit(solution)/shard_map/ppermute | solution.py:37
  32.2 9.8 %collective-permute-start.5 = (bf16[128,2048]{1,0:T(8,128)(2,1)S(1)}, bf16[128,2048]{1,0:T(8,128)(2,1)S(1)}, u32[]{:S(2)}, u32[]{:S(2)}) collective-permute-start(bf16[128,2048]{1,0:T(8,128)(2,1)S(1)} %collective-permute-done.4), channel_id=1, source_target_pairs={{1,0},{2,1},{3,2},{4,3},{5,4},{6,5},{7,6},{0,7},{9,8},{10,9},{11,1... | collective-permute-start | bytes 1572872 | tf_op jit(solution)/shard_map/ppermute | solution.py:44
  42.0 9.9 %collective-permute-start.3 = (bf16[128,2048]{1,0:T(8,128)(2,1)S(1)}, bf16[128,2048]{1,0:T(8,128)(2,1)}, u32[]{:S(2)}, u32[]{:S(2)}) collective-permute-start(bf16[128,2048]{1,0:T(8,128)(2,1)S(1)} %collective-permute-done.2), channel_id=1, source_target_pairs={{0,1},{1,2},{2,3},{3,4},{4,5},{5,6},{6,7},{7,0},{8,9},{9,10},{10,1... | collective-permute-start | bytes 1572872 | tf_op jit(solution)/shard_map/ppermute | solution.py:37
  42.0 16.9 %collective-permute-start.6 = (bf16[128,2048]{1,0:T(8,128)(2,1)S(1)}, bf16[128,2048]{1,0:T(8,128)(2,1)S(1)}, u32[]{:S(2)}, u32[]{:S(2)}) collective-permute-start(bf16[128,2048]{1,0:T(8,128)(2,1)S(1)} %collective-permute-done.5), channel_id=1, source_target_pairs={{1,0},{2,1},{3,2},{4,3},{5,4},{6,5},{7,6},{0,7},{9,8},{10,9},{11,1... | collective-permute-start | bytes 1572872 | tf_op jit(solution)/shard_map/ppermute | solution.py:44
Sparse Core Ops, SparseCore 0:
  11.1 99.4 all-gather.1
  131.2 38.7 reduce-scatter.1
